TPU v7x, 32 devices: a whole 2x2x4 slice. The times are simulated.
32 devices in a mesh: ep: 32 (over z, y, x, core).
Axes of the slice: x: 2, y: 2, z: 4, core: 2. Of those that a mesh axis runs over, the one named last changes fastest.
Arguments:
- tokens: bfloat16 [1024, 3072], P('ep'), may hold values from -6 to 6
- norm_gain: float32 [3072], replicated, may hold values from 0.1 to 1.9
- expert_ids: int32 [1024, 4], P('ep'), may hold values from 0 to 31, as said below
- expert_scores: float32 [1024, 4], P('ep'), may hold values from -100 to 180
- group_prob: float32 [1024], P('ep'), may hold values from 0.25 to 1
- gate_weight: bfloat16 [32, 3072, 384], P('ep'), may hold values from -0.109375 to 0.109375
- up_weight: bfloat16 [32, 3072, 384], P('ep'), may hold values from -0.109375 to 0.109375
- down_weight: bfloat16 [32, 384, 3072], P('ep'), may hold values from -0.3125 to 0.3125
Outputs:
- combined: bfloat16 [1024, 3072], P('ep')
Inputs may be any that keep to these rules, and one draw needn't show every extreme that they name: `expert_ids`: the 4 ids of a row are different and lie in one group of 8 consecutive experts. Among the rows of one device no expert is named by more than 16 rows, and in every draw some expert is named by exactly 16 rows of one device.
All inputs are finite; a program needn't handle non-finite values.
Results may differ from a plain program's by a relative error of at most 0.0085.
Values may be sent and summed in bfloat16 or wider, within the bound.
A program may use at most 128 MiB of HBM per device.

v0:
```python
import jax
import jax.numpy as jnp
from jax import lax
from jax.sharding import PartitionSpec as P

GROUPS = 4
TOP_K = 4


eps_norm = 1e-05


def layer_norm(tokens, norm_gain):
    values = tokens.astype(jnp.float32)
    average = jnp.mean(values, axis=1, keepdims=True)
    centred = values - average
    variance = jnp.mean(centred * centred, axis=1, keepdims=True)
    return (centred * lax.rsqrt(variance + eps_norm) * norm_gain[None, :]).astype(jnp.bfloat16)


def mixing_weights(expert_scores, group_prob):
    shifted = expert_scores - jnp.max(expert_scores, axis=1, keepdims=True)
    exp_scores = jnp.exp(shifted)
    return exp_scores / jnp.sum(exp_scores, axis=1, keepdims=True) * group_prob[:, None]


def expert_rows(flat_rows, gate_matrix, up_matrix, down_matrix):
    gate_act = jnp.dot(flat_rows, gate_matrix, preferred_element_type=jnp.float32)
    up_act = jnp.dot(flat_rows, up_matrix, preferred_element_type=jnp.float32)
    hidden = (jax.nn.silu(gate_act) * up_act).astype(jnp.bfloat16)
    return jnp.dot(hidden, down_matrix, preferred_element_type=jnp.float32).astype(jnp.bfloat16)


def local(
    tokens, norm_gain, expert_ids, expert_scores, group_prob, gate_weight, up_weight, down_weight
):
    normed = layer_norm(tokens, norm_gain)
    weights_tok = mixing_weights(expert_scores, group_prob)
    tok_count = tokens.shape[0]
    model_width = tokens.shape[1]
    expert_count = lax.axis_size("ep")
    group_size = expert_count // GROUPS
    capacity = (tok_count * TOP_K + group_size - 1) // group_size
    expert_iota = jnp.arange(expert_count, dtype=jnp.int32)
    slot_iota = jnp.arange(capacity, dtype=jnp.int32)
    matches = expert_ids[:, :, None] == expert_iota[None, None, :]
    route_weight = jnp.sum(jnp.where(matches, weights_tok[:, :, None], 0.0), axis=1)
    gate_matrix = gate_weight[0]
    up_matrix = up_weight[0]
    down_matrix = down_weight[0]
    chosen = jnp.sum(matches.astype(jnp.int32), axis=1)
    order_rank = jnp.cumsum(chosen, axis=0) - chosen
    slot_map = (chosen.T[:, None, :] == 1) & (order_rank.T[:, None, :] == slot_iota[None, :, None])
    outgoing = jnp.einsum(
        "emt,td->emd", slot_map.astype(jnp.bfloat16), normed, preferred_element_type=jnp.float32
    ).astype(jnp.bfloat16)
    received = lax.all_to_all(outgoing, "ep", split_axis=0, concat_axis=0, tiled=True)
    flat_rows = received.reshape(-1, model_width)
    results = expert_rows(flat_rows, gate_matrix, up_matrix, down_matrix).reshape(received.shape)
    returned_rows = lax.all_to_all(results, "ep", split_axis=0, concat_axis=0, tiled=True)
    slot_scale = jnp.where(slot_map, route_weight.T[:, None, :], 0.0)
    mixture = jnp.einsum(
        "emt,emd->td",
        slot_scale,
        returned_rows.astype(jnp.float32),
        precision=lax.Precision.HIGHEST,
    )
    return mixture.astype(jnp.bfloat16)


def solution(mesh):
    in_specs = (
        P("ep", None),
        P(),
        P("ep", None),
        P("ep", None),
        P("ep"),
        P("ep", None, None),
        P("ep", None, None),
        P("ep", None, None),
    )
    out_specs = P("ep", None)
    return jax.shard_map(local, mesh=mesh, in_specs=in_specs, out_specs=out_specs, check_vma=False)
```

profile of v0, /device:TPU:0, one launch (start us, length us, event | category | flops | bytes accessed | tf_op | source)
XLA Modules:
  0.0 176.0 jit_solution(9429624024677687291)
XLA Ops:
  0.0 0.0 copy-start
  0.0 0.9 convert_reduce_fusion.1
  0.9 0.1 reduce_window_sum.11
  1.1 0.2 copy.17
  1.2 1.1 convert_reduce_fusion
  2.3 1.2 fusion.22
  3.5 2.0 %convolution_convert_fusion.1 = bf16[32,16,3072]{2,1,0:T(8,128)(2,1)S(1)} fusion(pred[32,16,32]{2,1,0:T(8,128)(4,1)S(1)} %copy.17, bf16[32,3072]{1,0:T(8,128)(2,1)} %param.8, f32[3072]{0:T(1024)} %param.9, f32[32]{0:T(128)S(1)} %add_rsqrt_fusion, f32[32]{0:T(128)S(1)} %broadcast_multiply_fusion), kind=kOutput, calls=%fused_computation.1 | convolution fusion | flops 102727680 | bytes 3371264 | tf_op jit(solution)/shard_map/emt,td->emd/dot_general | solution.py:54
  5.5 0.0 copy-start.5
  5.5 78.3 %all_to_all.10 = bf16[32,16,3072]{2,1,0:T(8,128)(2,1)S(1)} all-to-all(bf16[32,16,3072]{2,1,0:T(8,128)(2,1)S(1)} %convolution_convert_fusion.1), channel_id=1, replica_groups=mesh['ep'=32] {'ep'}, dimensions={0} | all-to-all | bytes 6291456 | tf_op jit(solution)/shard_map/all_to_all | solution.py:57
  83.7 0.0 copy-start.1
  83.7 1.7 copy-done.1
  85.4 0.0 copy-done.5
  85.4 1.8 %fusion.5 = f32[512,384]{1,0:T(8,128)S(1)} fusion(bf16[512,3072]{1,0:T(8,128)(2,1)S(1)} %bitcast.33, bf16[1,3072,384]{2,1,0:T(8,128)(2,1)S(1)} %copy-done.5), kind=kOutput, calls=%fused_computation.8 | convolution fusion | flops 1207959552 | bytes 6291456 | tf_op jit(solution)/shard_map/dot_general | solution.py:28
  87.2 0.0 copy-done
  87.2 7.7 %convolution_convert_fusion = bf16[512,3072]{1,0:T(8,128)(2,1)} fusion(bf16[1,384,3072]{2,1,0:T(8,128)(2,1)S(1)} %copy-done, bf16[512,3072]{1,0:T(8,128)(2,1)} %bitcast.34, bf16[1,3072,384]{2,1,0:T(8,128)(2,1)} %param.14, f32[512,384]{1,0:T(8,128)S(1)} %fusion.5), kind=kOutput, calls=%fused_computation | convolution fusion | flops 2418671616 | bytes 11796480 | tf_op jit(solution)/shard_map/dot_general | solution.py:31
  95.0 0.0 copy-start.2
  95.0 0.0 copy-start.4
  95.0 0.0 copy-start.3
  95.0 3.8 %all-to-all-start.1 = ((bf16[32,16,3072]{2,1,0:T(8,128)(2,1)}), bf16[32,16,3072]{2,1,0:T(8,128)(2,1)}, u32[]{:S(2)}, u32[]{:S(2)}) async-start(bf16[32,16,3072]{2,1,0:T(8,128)(2,1)} %bitcast.32), calls=%async_computation.1 | async-start | bytes 6291456 | tf_op jit(solution)/shard_map/all_to_all | solution.py:60
  98.8 0.0 copy-done.2
  98.8 0.0 copy-done.4
  98.9 0.0 copy-done.3
  98.9 0.1 select_reduce_fusion
  99.0 71.1 %all-to-all-done.1 = bf16[32,16,3072]{2,1,0:T(8,128)(2,1)} async-done(((bf16[32,16,3072]{2,1,0:T(8,128)(2,1)}), bf16[32,16,3072]{2,1,0:T(8,128)(2,1)}, u32[]{:S(2)}, u32[]{:S(2)}) %all-to-all-start.1) | async-done | bytes 3145760 | tf_op jit(solution)/shard_map/all_to_all | solution.py:60
  170.1 5.9 %fusion = bf16[32,3072]{1,0:T(8,128)(2,1)} fusion(bf16[32,16,3072]{2,1,0:T(8,128)(2,1)} %all-to-all-done.1, f32[32,32]{0,1:T(8,128)S(1)} %bitcast.35, s32[32,32]{0,1:T(8,128)S(1)} %subtract_bitcast_fusion, pred[32,32]{0,1:T(8,128)(4,1)S(1)} %compare_bitcast_fusion), kind=kOutput, calls=%fused_computation.3 | convolution fusion | flops 604127232 | bytes 3351552 | tf_op jit(solution)/shard_map/emt,emd->td/dot_general | solution.py:62
  (8 shorter events, 0.1 us)
Async XLA Ops:
  0.0 87.2 %copy-start = (bf16[1,384,3072]{2,1,0:T(8,128)(2,1)S(1)}, bf16[1,384,3072]{2,1,0:T(8,128)(2,1)}, u32[]{:S(2)}) copy-start(bf16[1,384,3072]{2,1,0:T(8,128)(2,1)} %param.15) | copy-start | bytes 7077892
  5.5 80.0 %copy-start.5 = (bf16[1,3072,384]{2,1,0:T(8,128)(2,1)S(1)}, bf16[1,3072,384]{2,1,0:T(8,128)(2,1)}, u32[]{:S(2)}) copy-start(bf16[1,3072,384]{2,1,0:T(8,128)(2,1)} %param.13) | copy-start | bytes 7077892
  83.7 1.7 copy-start.1
  95.0 3.8 %copy-start.2 = (f32[32,4]{0,1:T(4,128)S(1)}, f32[32,4]{0,1:T(4,128)}, u32[]{:S(2)}) copy-start(f32[32,4]{0,1:T(4,128)} %param.11) | copy-start | bytes 1540
  95.0 3.8 %copy-start.4 = (f32[32]{0:T(128)S(1)}, f32[32]{0:T(128)}, u32[]{:S(2)}) copy-start(f32[32]{0:T(128)} %param.12) | copy-start | bytes 388
  95.0 3.9 %copy-start.3 = (s32[32,4]{0,1:T(4,128)S(1)}, s32[32,4]{0,1:T(4,128)}, u32[]{:S(2)}) copy-start(s32[32,4]{0,1:T(4,128)} %param.10) | copy-start | bytes 1540
  95.0 75.1 %all-to-all-start.1 = ((bf16[32,16,3072]{2,1,0:T(8,128)(2,1)}), bf16[32,16,3072]{2,1,0:T(8,128)(2,1)}, u32[]{:S(2)}, u32[]{:S(2)}) async-start(bf16[32,16,3072]{2,1,0:T(8,128)(2,1)} %bitcast.32), calls=%async_computation.1 | async-start | bytes 6291456 | tf_op jit(solution)/shard_map/all_to_all | solution.py:60
where the time goes:
time: 176 us
  blocking collectives  78.3 us (44%)
  waiting for transfers between devices  71.1 us (40%)
  matrix products  17.4 us (10%)
  starting transfers between devices  3.77 us (2%)
  other arithmetic  3.42 us (2%)
  local copies, waits for them, and re-layouts  1.91 us (1%)
    all_to_all x1, blocking collectives, local(): lax.all_to_all(outgoing, 'ep', split_axis=0, concat_axis=0, tiled=True)  78.3 us
    all_to_all x1, waiting for transfers between devices, local(): lax.all_to_all(results, 'ep', split_axis=0, concat_axis=0, tiled=True)  71.1 us
    dot_general x1, matrix products, expert_rows(): jnp.dot(hidden, down_matrix, preferred_element_type=jnp.float32)  7.74 us
    dot_general x1, matrix products, local(): jnp.einsum('emt,emd->td', slot_scale, returned_rows.astype(jnp.float32),...  5.89 us
    all_to_all x1, starting transfers between devices, local(): lax.all_to_all(results, 'ep', split_axis=0, concat_axis=0, tiled=True)  3.77 us
  transfers between devices with their start and end apart: 1, of which 1 were waited for; matrix products, arithmetic and copies ran while one was open for 0% of the time, Pallas kernels for 0%

commit v1 on v0

--- a/solution.py
+++ b/solution.py
@@ -36,36 +36,15 @@
 ):
     normed = layer_norm(tokens, norm_gain)
     weights_tok = mixing_weights(expert_scores, group_prob)
-    tok_count = tokens.shape[0]
-    model_width = tokens.shape[1]
     expert_count = lax.axis_size("ep")
-    group_size = expert_count // GROUPS
-    capacity = (tok_count * TOP_K + group_size - 1) // group_size
     expert_iota = jnp.arange(expert_count, dtype=jnp.int32)
-    slot_iota = jnp.arange(capacity, dtype=jnp.int32)
     matches = expert_ids[:, :, None] == expert_iota[None, None, :]
     route_weight = jnp.sum(jnp.where(matches, weights_tok[:, :, None], 0.0), axis=1)
-    gate_matrix = gate_weight[0]
-    up_matrix = up_weight[0]
-    down_matrix = down_weight[0]
-    chosen = jnp.sum(matches.astype(jnp.int32), axis=1)
-    order_rank = jnp.cumsum(chosen, axis=0) - chosen
-    slot_map = (chosen.T[:, None, :] == 1) & (order_rank.T[:, None, :] == slot_iota[None, :, None])
-    outgoing = jnp.einsum(
-        "emt,td->emd", slot_map.astype(jnp.bfloat16), normed, preferred_element_type=jnp.float32
-    ).astype(jnp.bfloat16)
-    received = lax.all_to_all(outgoing, "ep", split_axis=0, concat_axis=0, tiled=True)
-    flat_rows = received.reshape(-1, model_width)
-    results = expert_rows(flat_rows, gate_matrix, up_matrix, down_matrix).reshape(received.shape)
-    returned_rows = lax.all_to_all(results, "ep", split_axis=0, concat_axis=0, tiled=True)
-    slot_scale = jnp.where(slot_map, route_weight.T[:, None, :], 0.0)
-    mixture = jnp.einsum(
-        "emt,emd->td",
-        slot_scale,
-        returned_rows.astype(jnp.float32),
-        precision=lax.Precision.HIGHEST,
-    )
-    return mixture.astype(jnp.bfloat16)
+    rows = lax.all_gather(normed, "ep", axis=0, tiled=True)
+    own_weight = lax.all_to_all(route_weight.T, "ep", split_axis=0, concat_axis=0, tiled=True)
+    results = expert_rows(rows, gate_weight[0], up_weight[0], down_weight[0])
+    scaled = (results.astype(jnp.float32) * own_weight.reshape(-1)[:, None]).astype(jnp.bfloat16)
+    return lax.psum_scatter(scaled, "ep", scatter_dimension=0, tiled=True)
 
 
 def solution(mesh):

time: 176 us -> 223 us (1.27)
  waiting for transfers between devices: 71.1 us -> 167 us
  blocking collectives: 78.3 us -> 14.3 us
  between operations: 0.1 us -> 13.4 us
  other arithmetic: 3.42 us -> 7.62 us
  starting transfers between devices: 3.77 us -> 0.04 us
    reduce_scatter x0 -> x1, waiting for transfers between devices: none -> 114 us  [local(): return lax.psum_scatter(scaled, 'ep', scatter_dimension=0, tiled=True)]
    all_to_all x1 -> x0, waiting for transfers between devices: 71.1 us -> none  [local(): lax.all_to_all(results, 'ep', split_axis=0, concat_axis=0, tiled=True)]
    all_to_all x1, blocking collectives: 78.3 us -> 14.3 us  [local(): lax.all_to_all(route_weight.T, 'ep', split_axis=0, concat_axis=0, tiled=T...]
    all_gather x0 -> x1, waiting for transfers between devices: none -> 53.5 us  [local(): rows = lax.all_gather(normed, 'ep', axis=0, tiled=True)]
    dot_general x2 -> x0, matrix products: 7.85 us -> none  [the longest x1 5.89 us: local(): jnp.einsum('emt,emd->td', slot_scale, returned_rows.astype(jnp.float32),...]
    dot_general x1, matrix products: 1.78 us -> 8.08 us  [expert_rows(): jnp.dot(flat_rows, gate_matrix, preferred_element_type=jnp.float32)]
    all_to_all x1 -> x0, starting transfers between devices: 3.77 us -> none  [local(): lax.all_to_all(results, 'ep', split_axis=0, concat_axis=0, tiled=True)]
    dot_general x1, matrix products: 7.74 us -> 11.4 us  [expert_rows(): jnp.dot(hidden, down_matrix, preferred_element_type=jnp.float32)]
  transfers between devices with their start and end apart: 1 -> 2, of which waited for: 1 -> 2; matrix products, arithmetic and copies ran while one was open for 0% -> 2% of each run, Pallas kernels for 0% -> 0%
where the time goes in v1:
time: 223 us
  waiting for transfers between devices  167 us (75%)
  matrix products  19.5 us (9%)
  blocking collectives  14.3 us (6%)
  between operations  13.4 us (6%)
  other arithmetic  7.62 us (3%)
    reduce_scatter x1, waiting for transfers between devices, local(): return lax.psum_scatter(scaled, 'ep', scatter_dimension=0, tiled=True)  114 us
    all_gather x1, waiting for transfers between devices, local(): rows = lax.all_gather(normed, 'ep', axis=0, tiled=True)  53.5 us
    all_to_all x1, blocking collectives, local(): lax.all_to_all(route_weight.T, 'ep', split_axis=0, concat_axis=0, tiled=T...  14.3 us
    dot_general x1, matrix products, expert_rows(): jnp.dot(hidden, down_matrix, preferred_element_type=jnp.float32)  11.4 us
    dot_general x1, matrix products, expert_rows(): jnp.dot(flat_rows, gate_matrix, preferred_element_type=jnp.float32)  8.08 us
  transfers between devices with their start and end apart: 2, of which 2 were waited for; matrix products, arithmetic and copies ran while one was open for 2% of the time, Pallas kernels for 0%

profile of v1, /device:TPU:0, one launch (start us, length us, event | category | flops | bytes accessed | tf_op | source)
XLA Modules:
  0.0 222.7 jit_solution(8482960948131949265)
XLA Ops:
  6.5 0.0 copy-start
  6.5 0.0 all-gather.2.cloned.1.call-start
  6.5 1.2 convert_reduce_fusion
  7.8 1.2 fusion.11
  8.9 1.7 fusion.13
  10.7 0.0 all-gather.2.cloned.1.call-update
  10.7 0.0 reduce-scatter.2.cloned.1.call-start
  10.7 0.7 reduce_max.9
  11.4 0.7 fusion.14
  12.1 0.7 divide_multiply_fusion
  12.8 0.8 select_reduce_fusion
  13.6 0.1 copy.15
  13.7 14.3 %all_to_all.9 = f32[32,1,32]{2,1,0:T(1,128)S(1)} all-to-all(f32[32,1,32]{2,1,0:T(1,128)S(1)} %copy.15), channel_id=1, replica_groups=mesh['ep'=32] {'ep'}, dimensions={0} | all-to-all | bytes 8192 | tf_op jit(solution)/shard_map/all_to_all | solution.py:44
  28.0 0.5 broadcast.34
  28.5 0.6 reduce.3
  29.2 0.1 mul.53
  29.2 53.5 %all-gather.2.cloned.1.call-done = bf16[1024,3072]{1,0:T(8,128)(2,1)} async-done(((bf16[32,3072]{1,0:T(8,128)(2,1)}), bf16[1024,3072]{1,0:T(8,128)(2,1)}) %all-gather.2.cloned.1.call-update) | async-done | bytes 6291472 | tf_op jit(solution)/shard_map/all_gather | solution.py:43
  82.7 8.1 %fusion.3 = f32[1024,384]{1,0:T(8,128)} fusion(bf16[1024,3072]{1,0:T(8,128)(2,1)} %all-gather.2.cloned.1.call-done, bf16[1,3072,384]{2,1,0:T(8,128)(2,1)} %param.13), kind=kOutput, calls=%fused_computation.4 | convolution fusion | flops 2415919104 | bytes 10223616 | tf_op jit(solution)/shard_map/dot_general | solution.py:28
  90.8 0.0 copy-done
  90.8 11.4 %multiply_convert_fusion = bf16[1024,3072]{1,0:T(8,128)(2,1)} fusion(f32[1024]{0:T(1024)S(1)} %mul.53, bf16[1,384,3072]{2,1,0:T(8,128)(2,1)S(1)} %copy-done, f32[1024,384]{1,0:T(8,128)} %fusion.3, bf16[1024,3072]{1,0:T(8,128)(2,1)} %all-gather.2.cloned.1.call-done, bf16[1,3072,384]{2,1,0:T(8,128)(2,1)} %param.14), kind=kOutput, calls=%fused_computation | convolution fusion | flops 4846780416 | bytes 18878464 | tf_op jit(solution)/shard_map/dot_general | solution.py:31
  102.2 0.0 reduce-scatter.2.cloned.1.call-update
  102.2 113.7 %reduce-scatter.2.cloned.1.call-done = bf16[32,3072]{1,0:T(8,128)(2,1)} async-done(((bf16[1024,3072]{1,0:T(8,128)(2,1)}), bf16[32,3072]{1,0:T(8,128)(2,1)}) %reduce-scatter.2.cloned.1.call-update) | async-done | bytes 196624 | tf_op jit(solution)/shard_map/reduce_scatter | solution.py:47
  (2 shorter events, 0.0 us)
Async XLA Ops:
  6.5 84.3 %copy-start = (bf16[1,384,3072]{2,1,0:T(8,128)(2,1)S(1)}, bf16[1,384,3072]{2,1,0:T(8,128)(2,1)}, u32[]{:S(2)}) copy-start(bf16[1,384,3072]{2,1,0:T(8,128)(2,1)} %param.15) | copy-start | bytes 7077892
  6.5 76.2 %all-gather.2.cloned.1.call-start = ((), (), s32[]{:S(2)}) async-start(), calls=%async_computation.2 | async-start | bytes 6488064 | tf_op jit(solution)/shard_map/all_gather | solution.py:43
  10.7 205.2 %reduce-scatter.2.cloned.1.call-start = ((), (), s32[]{:S(2)}) async-start(), calls=%async_computation.3 | async-start | bytes 6488064 | tf_op jit(solution)/shard_map/reduce_scatter | solution.py:47
Sparse Core Ops, SparseCore 0:
  10.8 71.8 all-gather.1
  102.3 113.5 reduce-scatter.1

commit v2 on v0

--- a/solution.py
+++ b/solution.py
@@ -1,10 +1,16 @@
+import functools
+
 import jax
 import jax.numpy as jnp
 from jax import lax
+from jax.experimental import pallas as pl
+from jax.experimental.pallas import tpu as pltpu
 from jax.sharding import PartitionSpec as P
 
 GROUPS = 4
 TOP_K = 4
+LANES = 128
+MESH = pl.DeviceIdType.MESH
 
 
 eps_norm = 1e-05
@@ -67,6 +73,317 @@
     )
     return mixture.astype(jnp.bfloat16)
 
+def ring_kernel(
+    zs, tok_ref, gain_ref, ids_ref, score_ref, prob_ref, gate_hbm, up_hbm, down_hbm, out_ref,
+    x0, x1, p0, p1, rd0, rd1, rb0, rb1, ra0, ra1, rz0, rz1, wg, wu, wd, w_sem,
+    gather_recv, gather_pair_recv, gather_z, gather_x, gather_y, gather_pair,
+    pair_recv, pair_send, far_recv, far_send, near_recv, near_send, line_recv, line_send,
+):
+    xs, ps, rds, rbs, ras, rzs = (x0, x1), (p0, p1), (rd0, rd1), (rb0, rb1), (ra0, ra1), (rz0, rz1)
+    me = lax.axis_index("ep")
+    core = lax.rem(me, 2)
+    x = lax.rem(lax.div(me, 2), 2)
+    y = lax.rem(lax.div(me, 4), 2)
+    z = lax.div(me, 8)
+
+    def device(zz, yy, xx, cc):
+        return ((zz * 2 + yy) * 2 + xx) * 2 + cc
+
+    partner = device(z, y, x, 1 - core)
+    x_side = device(z, y, 1 - x, core)
+    y_side = device(z, 1 - y, x, core)
+    z_side = (device(z - 1, y, x, core), device(z + 1, y, x, core))
+    has = (z > 0, z < zs - 1)
+    chunks = [yy * 2 + xx for yy in (y, 1 - y) for xx in (x, 1 - x)]
+
+    def base(rel, cc):
+        return (chunks[rel] * 2 + cc) * zs
+
+    copies = [
+        pltpu.make_async_copy(src.at[0], dst, w_sem.at[i])
+        for i, (src, dst) in enumerate(((gate_hbm, wg), (up_hbm, wu), (down_hbm, wd)))
+    ]
+    for copy in copies:
+        copy.start()
+
+    barrier = pltpu.get_barrier_semaphore()
+    for other in (partner, x_side, y_side):
+        pl.semaphore_signal(barrier, inc=1, device_id=(other,), device_id_type=MESH)
+    for d in (0, 1):
+        @pl.when(has[d])
+        def _():
+            pl.semaphore_signal(barrier, inc=1, device_id=(z_side[d],), device_id_type=MESH)
+
+    model_width = tok_ref.shape[1]
+    half = x0.shape[2]
+    values = tok_ref[...].astype(jnp.float32)
+    average = jnp.sum(values, axis=1, keepdims=True) * (1.0 / model_width)
+    centred = values - average
+    variance = jnp.sum(centred * centred, axis=1, keepdims=True) * (1.0 / model_width)
+    normed = (centred * lax.rsqrt(variance + eps_norm) * gain_ref[...]).astype(jnp.bfloat16)
+    score = [score_ref[:, k : k + 1] for k in range(TOP_K)]
+    top = functools.reduce(jnp.maximum, score)
+    exps = [jnp.exp(s - top) for s in score]
+    total = functools.reduce(jnp.add, exps)
+    lane = lax.broadcasted_iota(jnp.int32, (tok_ref.shape[0], LANES), 1)
+    meta = jnp.zeros((tok_ref.shape[0], LANES), jnp.float32)
+    for k in range(TOP_K):
+        weight = exps[k] / total * prob_ref[...]
+        high = weight.astype(jnp.bfloat16).astype(jnp.float32)
+        meta = jnp.where(lane == k, ids_ref[:, k : k + 1].astype(jnp.float32), meta)
+        meta = jnp.where(lane == TOP_K + k, high, meta)
+        meta = jnp.where(lane == 2 * TOP_K + k, weight - high, meta)
+    own = base(0, core) + z
+    x0[own] = normed[:, :half]
+    x1[own, :, : model_width - half] = normed[:, half:]
+    x1[own, :, model_width - half :] = meta.astype(jnp.bfloat16)
+
+    inside = jnp.logical_and(has[0], has[1])
+
+    @pl.when(inside)
+    def _():
+        pl.semaphore_wait(barrier, 5)
+
+    @pl.when(jnp.logical_not(inside))
+    def _():
+        pl.semaphore_wait(barrier, 4)
+
+    pending = []
+
+    def send(src, dst, send_sem, recv_sem, target, conds=()):
+        array, index = send_sem
+        pltpu.make_async_remote_copy(
+            src_ref=src(), dst_ref=dst(), send_sem=array.at[index], recv_sem=recv_sem,
+            device_id=(target,), device_id_type=MESH,
+        ).start()
+
+        def finish():
+            sem = array.at[index]
+            pltpu.make_async_remote_copy(
+                src_ref=src(), dst_ref=dst(), send_sem=sem, recv_sem=sem,
+                device_id=(target,), device_id_type=MESH,
+            ).wait_send()
+
+        pending.append((conds, finish))
+
+    def landed(dst, recv_sem):
+        pltpu.make_async_remote_copy(
+            src_ref=dst, dst_ref=dst, send_sem=recv_sem, recv_sem=recv_sem,
+            device_id=(partner,), device_id_type=MESH,
+        ).wait_recv()
+
+    def at_distance(s, body):
+        if s == 0:
+            body(z, (), None)
+            return
+        for d, q, ok in ((1, z - s, z - s >= 0), (0, z + s, z + s < zs)):
+            @pl.when(ok)
+            def _():
+                body(q, (ok,), d)
+
+    def spread(q, conds, came):
+        for h in (0, 1):
+            block = functools.partial(lambda h: xs[h].at[base(0, core) + q], h)
+            if came is not None:
+                landed(block(), gather_recv.at[h, 0, q])
+            for d in (0, 1):
+                if came is None or came == d:
+                    @pl.when(has[d])
+                    def _():
+                        send(block, block, (gather_z, (h, d, q)), gather_recv.at[h, 0, q],
+                             z_side[d], conds + (has[d],))
+            send(block, block, (gather_x, (h, 0, q)), gather_recv.at[h, 1, q], x_side, conds)
+            send(block, block, (gather_y, (h, 0, q)), gather_recv.at[h, 2, q], y_side, conds)
+
+    def forward(q, conds, _):
+        block = lambda: x0.at[base(1, core) + q]
+        landed(block(), gather_recv.at[0, 1, q])
+        send(block, block, (gather_y, (0, 1, q)), gather_recv.at[0, 3, q], y_side, conds)
+        other = lambda: x1.at[base(2, core) + q]
+        landed(other(), gather_recv.at[1, 2, q])
+        send(other, other, (gather_x, (1, 1, q)), gather_recv.at[1, 3, q], x_side, conds)
+
+    def all_landed(h, rel):
+        for q in range(zs):
+            landed(xs[h].at[base(rel, core) + q], gather_recv.at[h, rel, q])
+
+    def pair_gather(rel):
+        for h in (0, 1):
+            blocks = functools.partial(lambda h: xs[h].at[pl.ds(base(rel, core), zs)], h)
+            send(blocks, blocks, (gather_pair, (h, rel)), gather_pair_recv.at[h, rel], partner)
+
+    def compute(rel):
+        for h in (0, 1):
+            landed(xs[h].at[pl.ds(base(rel, 1 - core), zs)], gather_pair_recv.at[h, rel])
+        slots = pl.ds(chunks[rel] * 2 * zs, 2 * zs)
+        rows = 2 * zs * tok_ref.shape[0]
+        left = x0[slots].reshape(rows, half)
+        right = x1[slots, :, : model_width - half].reshape(rows, model_width - half)
+        tags = x1[slots, :, model_width - half :].reshape(rows, LANES).astype(jnp.float32)
+        expert = me.astype(jnp.float32)
+        scale = jnp.zeros((rows, 1), jnp.float32)
+        for k in range(TOP_K):
+            value = tags[:, TOP_K + k : TOP_K + k + 1] + tags[:, 2 * TOP_K + k : 2 * TOP_K + k + 1]
+            scale += jnp.where(tags[:, k : k + 1] == expert, value, 0.0)
+
+        def project(w):
+            return jnp.dot(left, w[:half, :], preferred_element_type=jnp.float32) + jnp.dot(
+                right, w[half:, :], preferred_element_type=jnp.float32
+            )
+
+        gate_act = project(wg)
+        up_act = project(wu)
+        hidden = (jax.nn.silu(gate_act) * up_act).astype(jnp.bfloat16)
+        step = half // 3 if half % (3 * LANES) == 0 else half
+        for h in (0, 1):
+            width = ps[h].shape[2]
+            for at in range(0, width, step):
+                part = jnp.dot(hidden, wd[:, h * half + at : h * half + at + step],
+                               preferred_element_type=jnp.float32)
+                part = (part.astype(jnp.bfloat16).astype(jnp.float32) * scale).astype(jnp.bfloat16)
+                ps[h][slots, :, at : at + step] = part.reshape(2 * zs, tok_ref.shape[0], step)
+
+    def pair_reduce(rel):
+        for h in (0, 1):
+            part = functools.partial(lambda h: ps[h].at[pl.ds(base(rel, 1 - core), zs)], h)
+            room = functools.partial(lambda h: rds[h].at[rel], h)
+            send(part, room, (pair_send, (h, rel)), pair_recv.at[h, rel], partner)
+
+    def pair_add(rel):
+        for h in (0, 1):
+            landed(rds[h].at[rel], pair_recv.at[h, rel])
+            slots = pl.ds(base(rel, core), zs)
+            ps[h][slots] = ps[h][slots] + rds[h][rel]
+
+    far_side = (y_side, x_side)
+    near_side = (x_side, y_side)
+
+    def far(h, rel, kind):
+        def body(q, conds, _):
+            send(lambda: ps[h].at[base(rel, core) + q], lambda: rbs[h].at[kind, q],
+                 (far_send, (h, kind, q)), far_recv.at[h, kind, q], far_side[h], conds)
+        return body
+
+    def near(q, conds, _):
+        for h in (0, 1):
+            landed(rbs[h].at[1, q], far_recv.at[h, 1, q])
+            slot = base(1 + h, core) + q
+            ps[h][slot] = ps[h][slot] + rbs[h][1, q]
+            part = functools.partial(lambda h: ps[h].at[base(1 + h, core) + q], h)
+            room = functools.partial(lambda h: ras[h].at[q], h)
+            send(part, room, (near_send, (h, q)), near_recv.at[h, q],
+                 near_side[h], conds)
+
+    def line(q, conds, d):
+        for h in (0, 1):
+            landed(rbs[h].at[0, q], far_recv.at[h, 0, q])
+            landed(ras[h].at[q], near_recv.at[h, q])
+            slot = base(0, core) + q
+            held = ps[h][slot].astype(jnp.float32) + rbs[h][0, q].astype(jnp.float32)
+            ps[h][slot] = (held + ras[h][q].astype(jnp.float32)).astype(jnp.bfloat16)
+            if d is None:
+                for side in (0, 1):
+                    @pl.when(has[side])
+                    def _():
+                        landed(rzs[h].at[side, q], line_recv.at[h, side, q])
+                        ps[h][slot] = ps[h][slot] + rzs[h][side, q]
+                width = ps[h].shape[2]
+                out_ref[:, h * half : h * half + width] = ps[h][slot]
+            else:
+                @pl.when(has[d])
+                def _():
+                    landed(rzs[h].at[d, q], line_recv.at[h, d, q])
+                    ps[h][slot] = ps[h][slot] + rzs[h][d, q]
+                part = functools.partial(lambda h: ps[h].at[base(0, core) + q], h)
+                room = functools.partial(lambda h: rzs[h].at[d, q], h)
+                send(part, room, (line_send, (h, d, q)),
+                     line_recv.at[h, d, q], z_side[1 - d], conds)
+
+    def far_first(body):
+        for s in range(zs - 1, -1, -1):
+            at_distance(s, body)
+
+    at_distance(0, spread)
+    for s in range(1, zs):
+        at_distance(s, spread)
+        at_distance(s - 1, forward)
+    pair_gather(0)
+    for copy in copies:
+        copy.wait()
+    compute(0)
+    pair_reduce(0)
+    at_distance(zs - 1, forward)
+    all_landed(1, 1)
+    pair_gather(1)
+    all_landed(0, 2)
+    pair_gather(2)
+    compute(1)
+    pair_reduce(1)
+    compute(2)
+    pair_reduce(2)
+    pair_add(1)
+    far_first(far(1, 1, 0))
+    pair_add(2)
+    far_first(far(0, 2, 0))
+    for h in (0, 1):
+        all_landed(h, 3)
+    pair_gather(3)
+    compute(3)
+    pair_reduce(3)
+    pair_add(0)
+    pair_add(3)
+    far_first(far(0, 3, 1))
+    far_first(far(1, 3, 1))
+    at_distance(zs - 1, near)
+    for s in range(zs - 2, -1, -1):
+        at_distance(s, near)
+        at_distance(s + 1, line)
+    at_distance(0, line)
+
+    for conds, finish in pending:
+        if conds:
+            pl.when(functools.reduce(jnp.logical_and, conds))(finish)
+        else:
+            finish()
+
+
+def ring_local(
+    zs, tokens, norm_gain, expert_ids, expert_scores, group_prob, gate_weight, up_weight, down_weight
+):
+    count, width = tokens.shape
+    hidden = gate_weight.shape[2]
+    slots = zs * 8
+    half = width // 2
+    kind = jnp.bfloat16
+    vmem = pl.BlockSpec(memory_space=pltpu.VMEM)
+    hbm = pl.BlockSpec(memory_space=pl.ANY)
+    dma = pltpu.SemaphoreType.DMA
+    widths = (half, width - half)
+    each = lambda *lead: [pltpu.VMEM(lead + (count, w), kind) for w in widths]
+    scratch = [
+        pltpu.VMEM((slots, count, half), kind),
+        pltpu.VMEM((slots, count, width - half + LANES), kind),
+        *each(slots), *each(4, zs), *each(2, zs), *each(zs), *each(2, zs),
+        pltpu.VMEM((width, hidden), kind), pltpu.VMEM((width, hidden), kind),
+        pltpu.VMEM((hidden, width), kind), dma((3,)),
+        dma((2, 4, zs)), dma((2, 4)), dma((2, 2, zs)), dma((2, 2, zs)), dma((2, 2, zs)), dma((2, 4)),
+        dma((2, 4)), dma((2, 4)), dma((2, 2, zs)), dma((2, 2, zs)),
+        dma((2, zs)), dma((2, zs)), dma((2, 2, zs)), dma((2, 2, zs)),
+    ]
+    return pl.pallas_call(
+        functools.partial(ring_kernel, zs),
+        out_shape=jax.ShapeDtypeStruct((count, width), kind),
+        in_specs=[vmem] * 5 + [hbm] * 3,
+        out_specs=vmem,
+        scratch_shapes=scratch,
+        compiler_params=pltpu.CompilerParams(
+            collective_id=0, has_side_effects=True, vmem_limit_bytes=60 * 1024 * 1024
+        ),
+    )(
+        tokens, norm_gain[None, :], expert_ids, expert_scores, group_prob[:, None],
+        gate_weight, up_weight, down_weight,
+    )
+
 
 def solution(mesh):
     in_specs = (
@@ -80,4 +397,6 @@
         P("ep", None, None),
     )
     out_specs = P("ep", None)
-    return jax.shard_map(local, mesh=mesh, in_specs=in_specs, out_specs=out_specs, check_vma=False)
+    devices = mesh.shape["ep"]
+    body = functools.partial(ring_local, GROUPS) if devices == GROUPS * 8 else local
+    return jax.shard_map(body, mesh=mesh, in_specs=in_specs, out_specs=out_specs, check_vma=False)

time: 176 us -> 83.5 us (0.47)
  blocking collectives: 78.3 us -> 0 us
  Pallas kernels: 0 us -> 77.6 us
  waiting for transfers between devices: 71.1 us -> 0 us
  matrix products: 17.4 us -> 0 us
  starting transfers between devices: 3.77 us -> 0 us
  local copies, waits for them, and re-layouts: 1.91 us -> 5.67 us
  other arithmetic: 3.42 us -> 0 us
    all_to_all x1 -> x0, blocking collectives: 78.3 us -> none  [local(): lax.all_to_all(outgoing, 'ep', split_axis=0, concat_axis=0, tiled=True)]
    pallas_call x0 -> x1, Pallas kernels: none -> 77.6 us  [ring_local(): pl.pallas_call(functools.partial(ring_kernel, zs), out_shape=jax.ShapeDty...]
    all_to_all x1 -> x0, waiting for transfers between devices: 71.1 us -> none  [local(): lax.all_to_all(results, 'ep', split_axis=0, concat_axis=0, tiled=True)]
    dot_general x4 -> x0, matrix products: 17.4 us -> none  [the longest x1 7.74 us: expert_rows(): jnp.dot(hidden, down_matrix, preferred_element_type=jnp.float32)]
    all_to_all x1 -> x0, starting transfers between devices: 3.77 us -> none  [local(): lax.all_to_all(results, 'ep', split_axis=0, concat_axis=0, tiled=True)]
    reduce_sum x5 -> x0, other arithmetic: 3.26 us -> none  [the longest x1 1.16 us: layer_norm(): variance = jnp.mean(centred * centred, axis=1, keepdims=True)]
    unnamed x12 -> x3, local copies, waits for them, and re-layouts: 1.72 us -> 4.34 us
  transfers between devices with their start and end apart: 1 -> 0, of which waited for: 1 -> 0; matrix products, arithmetic and copies ran while one was open for 0% -> 0% of each run, Pallas kernels for 0% -> 0%
where the time goes in v2:
time: 83.5 us; the launch traced here: 83.2 us
  Pallas kernels  77.6 us (93%)
  local copies, waits for them, and re-layouts  5.67 us (7%)
    pallas_call x1, Pallas kernels, ring_local(): pl.pallas_call(functools.partial(ring_kernel, zs), out_shape=jax.ShapeDty...  77.6 us
    unnamed x3, local copies, waits for them, and re-layouts  4.34 us

profile of v2, /device:TPU:0, one launch (start us, length us, event | category | flops | bytes accessed | tf_op | source)
XLA Modules:
  0.0 83.2 jit_solution(3197972909398340140)
XLA Ops:
  0.0 1.4 %copy.9.ids_ref = s32[32,4]{1,0:T(8,128)} copy(s32[32,4]{0,1:T(4,128)} %param.10) | data formatting | bytes 1024 | tf_op args[2]
  1.4 1.4 %copy.10.score_ref = f32[32,4]{1,0:T(8,128)} copy(f32[32,4]{0,1:T(4,128)} %param.11) | data formatting | bytes 1024 | tf_op args[3]
  2.7 1.3 %copy.11.prob_ref = f32[32,1]{1,0:T(8,128)} copy(f32[32,1]{0,1:T(1,128)} %bitcast.3) | data formatting | bytes 256 | tf_op jit(solution)/shard_map/broadcast_in_dim | solution.py:383
  4.1 77.6 %shard_map.82 = bf16[32,3072]{1,0:T(8,128)(2,1)} custom-call(bf16[32,3072]{1,0:T(8,128)(2,1)} %tok_ref.1, f32[1,3072]{1,0:T(1,128)} %bitcast.2, s32[32,4]{1,0:T(8,128)} %copy.9.ids_ref, f32[32,4]{1,0:T(8,128)} %copy.10.score_ref, f32[32,1]{1,0:T(8,128)} %copy.11.prob_ref, bf16[1,3072,384]{2,1,0:T(8,128)(2,1)} %gate_hbm.1, bf16[1,3072,384]{2,1,0:T(8,128)(2,1)} %up_hbm.1, ...), custom_call_target="tpu_custom_call" | custom-call | tf_op jit(solution)/shard_map/pallas_call | solution.py:373
  81.6 1.6 %copy.13 = bf16[32,3072]{1,0:T(8,128)(2,1)} copy(bf16[32,3072]{1,0:T(8,128)(2,1)} %shard_map.82) | data formatting | bytes 393216

commit v3 on v2

--- a/solution.py
+++ b/solution.py
@@ -121,18 +121,25 @@
     centred = values - average
     variance = jnp.sum(centred * centred, axis=1, keepdims=True) * (1.0 / model_width)
     normed = (centred * lax.rsqrt(variance + eps_norm) * gain_ref[...]).astype(jnp.bfloat16)
-    score = [score_ref[:, k : k + 1] for k in range(TOP_K)]
+    count = tok_ref.shape[0]
+    score = [score_ref[k : k + 1, :] for k in range(TOP_K)]
     top = functools.reduce(jnp.maximum, score)
     exps = [jnp.exp(s - top) for s in score]
     total = functools.reduce(jnp.add, exps)
-    lane = lax.broadcasted_iota(jnp.int32, (tok_ref.shape[0], LANES), 1)
-    meta = jnp.zeros((tok_ref.shape[0], LANES), jnp.float32)
+    row = lax.broadcasted_iota(jnp.int32, (LANES, count), 0)
+    tags = jnp.zeros((LANES, count), jnp.float32)
     for k in range(TOP_K):
         weight = exps[k] / total * prob_ref[...]
         high = weight.astype(jnp.bfloat16).astype(jnp.float32)
-        meta = jnp.where(lane == k, ids_ref[:, k : k + 1].astype(jnp.float32), meta)
-        meta = jnp.where(lane == TOP_K + k, high, meta)
-        meta = jnp.where(lane == 2 * TOP_K + k, weight - high, meta)
+        tags = jnp.where(row == k, ids_ref[k : k + 1, :].astype(jnp.float32), tags)
+        tags = jnp.where(row == TOP_K + k, high, tags)
+        tags = jnp.where(row == 2 * TOP_K + k, weight - high, tags)
+    square = (count, count)
+    same = lax.broadcasted_iota(jnp.int32, square, 0) == lax.broadcasted_iota(jnp.int32, square, 1)
+    meta = lax.dot_general(
+        same.astype(jnp.float32).astype(jnp.bfloat16), tags.astype(jnp.bfloat16),
+        (((1,), (1,)), ((), ())), preferred_element_type=jnp.float32,
+    )
     own = base(0, core) + z
     x0[own] = normed[:, :half]
     x1[own, :, : model_width - half] = normed[:, half:]
@@ -319,10 +326,11 @@
     pair_gather(2)
     compute(1)
     pair_reduce(1)
+    pair_add(1)
+    far_first(far(1, 1, 0))
     compute(2)
     pair_reduce(2)
-    pair_add(1)
-    far_first(far(1, 1, 0))
+    pair_add(0)
     pair_add(2)
     far_first(far(0, 2, 0))
     for h in (0, 1):
@@ -330,7 +338,6 @@
     pair_gather(3)
     compute(3)
     pair_reduce(3)
-    pair_add(0)
     pair_add(3)
     far_first(far(0, 3, 1))
     far_first(far(1, 3, 1))
@@ -380,8 +387,7 @@
             collective_id=0, has_side_effects=True, vmem_limit_bytes=60 * 1024 * 1024
         ),
     )(
-        tokens, norm_gain[None, :], expert_ids, expert_scores, group_prob[:, None],
-        gate_weight, up_weight, down_weight,
+        tokens, norm_gain[None, :], expert_ids.T, expert_scores.T, group_prob[None, :], gate_weight, up_weight, down_weight,
     )
 
 

time: 83.5 us -> 79.9 us (0.957)
  local copies, waits for them, and re-layouts: 5.67 us -> 1.62 us
    unnamed x3 -> x1, local copies, waits for them, and re-layouts: 4.34 us -> 1.62 us
    broadcast_in_dim x1 -> x0, local copies, waits for them, and re-layouts: 1.33 us -> none  [ring_local(): group_prob[:, None]]
where the time goes in v3:
time: 79.9 us; the launch traced here: 79.5 us
  Pallas kernels  77.9 us (97%)
  local copies, waits for them, and re-layouts  1.62 us (2%)
    pallas_call x1, Pallas kernels, ring_local(): pl.pallas_call(functools.partial(ring_kernel, zs), out_shape=jax.ShapeDty...  77.9 us
    unnamed x1, local copies, waits for them, and re-layouts  1.62 us

profile of v3, /device:TPU:0, one launch (start us, length us, event | category | flops | bytes accessed | tf_op | source)
XLA Modules:
  0.0 79.5 jit_solution(17802242280412603456)
XLA Ops:
  0.0 77.9 %shard_map.82 = bf16[32,3072]{1,0:T(8,128)(2,1)} custom-call(bf16[32,3072]{1,0:T(8,128)(2,1)} %tok_ref.1, f32[1,3072]{1,0:T(1,128)} %bitcast.4, s32[4,32]{1,0:T(4,128)} %bitcast.5, f32[4,32]{1,0:T(4,128)} %bitcast.6, f32[1,32]{1,0:T(1,128)} %bitcast.7, bf16[1,3072,384]{2,1,0:T(8,128)(2,1)} %gate_hbm.1, bf16[1,3072,384]{2,1,0:T(8,128)(2,1)} %up_hbm.1, ...), custom_call_target="tpu_custom_call" | custom-call | tf_op jit(solution)/shard_map/pallas_call | solution.py:380
  77.9 1.6 %copy.10 = bf16[32,3072]{1,0:T(8,128)(2,1)} copy(bf16[32,3072]{1,0:T(8,128)(2,1)} %shard_map.82) | data formatting | bytes 393216
